TPU v7x, 32 devices: a whole 2x2x4 slice. The times are simulated.
32 devices in a mesh: sp: 8 (over z, x), tp: 4 (over y, core).
Axes of the slice: x: 2, y: 2, z: 4, core: 2. Of those that a mesh axis runs over, the one named last changes fastest.
Arguments:
- queries: bfloat16 [4096, 2048], P('sp', 'tp'), may hold values from -90 to 90, as said below
- key_rows: bfloat16 [4096, 512], P('sp', 'tp'), may hold values from -6 to 6
- value_rows: bfloat16 [4096, 512], P('sp', 'tp'), may hold values from -6 to 6
- sink_logits: float32 [16], P('tp'), may hold values from 2 to 7
- residual: bfloat16 [4096, 2048], P('sp'), may hold values from -6 to 6
- norm_gain: float32 [2048], replicated, may hold values from 0.1 to 1.9
- out_weight: bfloat16 [2048, 2048], P('tp'), may hold values from -1.5 to 1.5
- gate_weight: bfloat16 [2048, 5632], P('sp', 'tp'), may hold values from -0.125 to 0.125
- up_weight: bfloat16 [2048, 5632], P('sp', 'tp'), may hold values from -0.125 to 0.125
- down_weight: bfloat16 [5632, 2048], P('tp', 'sp'), may hold values from -0.078125 to 0.078125
Outputs:
- mixed: bfloat16 [4096, 2048], P(('sp', 'tp'))
Inputs may be any that keep to these rules, and one draw needn't show every extreme that they name: queries are mostly of order one; some rows may be much larger.
All inputs are finite; a program needn't handle non-finite values.
Results may differ from a plain program's by a relative error of at most 0.012.
Values may be sent and summed in bfloat16 or wider, within the bound.
A program may use at most 128 MiB of HBM per device.

v0:
```python
import jax
import jax.numpy as jnp
from jax import lax
from jax.sharding import PartitionSpec as P

DH = 128
WIN = 128
EPSILON = 1e-06
MASKED = -1e30


def with_halo(cells, sides, width):
    for axis, dim in sides:
        count = lax.axis_size(axis)
        ends = count - 1
        head = lax.slice_in_dim(cells, 0, width, axis=dim)
        tail = lax.slice_in_dim(cells, cells.shape[dim] - width, cells.shape[dim], axis=dim)
        cells = jnp.concatenate(
            [
                lax.ppermute(tail, axis, [(i, (i + 1) % count) for i in range(ends)]),
                cells,
                lax.ppermute(head, axis, [((i + 1) % count, i) for i in range(ends)]),
            ],
            axis=dim,
        )
    return cells


def attend_block(query_blk, key_blk, value_blk, sink_logits, query_pos, key_pos, seq_len):
    kv_heads = key_blk.shape[1] // DH
    group_size = query_blk.shape[1] // key_blk.shape[1]
    query_four = query_blk.reshape(query_blk.shape[0], kv_heads, group_size, DH)
    key_three = key_blk.reshape(key_blk.shape[0], kv_heads, DH)
    value_three = value_blk.reshape(value_blk.shape[0], kv_heads, DH)
    scores = jnp.einsum(
        "qhgd,khd->hgqk", query_four, key_three, preferred_element_type=jnp.float32
    ) * DH ** (-0.5)
    allowed = (
        (jnp.abs(key_pos[None, :] - query_pos[:, None]) <= WIN)
        & (key_pos[None, :] >= 0)
        & (key_pos[None, :] < seq_len)
    )
    scores = jnp.where(allowed[None, None], scores, MASKED)
    sink_col = sink_logits.reshape(kv_heads, group_size)[:, :, None]
    highest = jnp.maximum(jnp.max(scores, axis=-1), sink_col)
    weights_exp = jnp.exp(scores - highest[..., None])
    denominator = jnp.sum(weights_exp, axis=-1) + jnp.exp(sink_col - highest)
    probabilities = (weights_exp / denominator[..., None]).astype(jnp.bfloat16)
    heads_out = jnp.einsum(
        "hgqk,khd->qhgd", probabilities, value_three, preferred_element_type=jnp.float32
    )
    return heads_out.astype(jnp.bfloat16).reshape(query_blk.shape[0], kv_heads * group_size * DH)


def rms_scale(rows_wide, norm_gain):
    mean_square = jnp.mean(rows_wide * rows_wide, axis=-1, keepdims=True)
    return (rows_wide * lax.rsqrt(mean_square + EPSILON) * norm_gain).astype(jnp.bfloat16)


def fetch_down(down_weight):
    return lax.all_gather(down_weight, "sp", axis=1, tiled=True)


def shards(
    queries,
    key_rows,
    value_rows,
    sink_logits,
    residual,
    norm_gain,
    out_weight,
    gate_weight,
    up_weight,
    down_weight,
):
    tok_local = queries.shape[0]
    block_len = 2 * WIN
    share_rows = tok_local // lax.axis_size("tp")
    seq_len = tok_local * lax.axis_size("sp")
    device_offset = lax.axis_index("sp") * tok_local
    kv_pair = jnp.stack([key_rows, value_rows])
    kv_ext = with_halo(kv_pair, (("sp", 1),), WIN)

    def one_block(block_index):
        block_first = block_index * block_len
        query_blk = lax.dynamic_slice_in_dim(queries, block_first, block_len, 0)
        key_blk = lax.dynamic_slice_in_dim(kv_ext[0], block_first, block_len + 2 * WIN, 0)
        value_blk = lax.dynamic_slice_in_dim(kv_ext[1], block_first, block_len + 2 * WIN, 0)
        query_pos = device_offset + block_first + jnp.arange(block_len, dtype=jnp.int32)
        key_pos = (
            device_offset + block_first - WIN + jnp.arange(block_len + 2 * WIN, dtype=jnp.int32)
        )
        return attend_block(query_blk, key_blk, value_blk, sink_logits, query_pos, key_pos, seq_len)

    blocks = lax.map(one_block, jnp.arange(tok_local // block_len, dtype=jnp.int32))
    attended = blocks.reshape(tok_local, queries.shape[1])
    own_first = lax.axis_index("tp") * share_rows
    attn_full = lax.psum(
        jnp.dot(attended, out_weight, preferred_element_type=jnp.float32).astype(jnp.bfloat16), "tp"
    ).astype(jnp.float32)
    middle_all = residual.astype(jnp.float32) + attn_full
    normed_all = rms_scale(middle_all, norm_gain)
    middle_own = lax.dynamic_slice_in_dim(middle_all, own_first, share_rows, 0)
    gate_sectioned = lax.all_gather(gate_weight, "sp", axis=0, tiled=True)
    up_sectioned = lax.all_gather(up_weight, "sp", axis=0, tiled=True)
    gate_acc = jnp.dot(normed_all, gate_sectioned, preferred_element_type=jnp.float32)
    up_acc = jnp.dot(normed_all, up_sectioned, preferred_element_type=jnp.float32)
    down_whole = fetch_down(down_weight)
    hidden = (jax.nn.silu(gate_acc) * up_acc).astype(jnp.bfloat16)
    ffn_share = lax.psum_scatter(
        jnp.dot(hidden, down_whole, preferred_element_type=jnp.float32).astype(jnp.bfloat16),
        "tp",
        scatter_dimension=0,
        tiled=True,
    ).astype(jnp.float32)
    return (middle_own + ffn_share).astype(jnp.bfloat16)


def solution(mesh):
    placed = (
        P("sp", "tp"),
        P("sp", "tp"),
        P("sp", "tp"),
        P("tp"),
        P("sp", None),
        P(),
        P("tp", None),
        P("sp", "tp"),
        P("sp", "tp"),
        P("tp", "sp"),
    )
    return jax.shard_map(
        shards, mesh=mesh, in_specs=placed, out_specs=P(("sp", "tp"), None), check_vma=False
    )
```

profile of v0, /device:TPU:0, one launch (start us, length us, event | category | flops | bytes accessed | tf_op | source)
XLA Modules:
  0.0 370.6 jit_solution(8707252518556242722)
XLA Ops:
  7.4 1.0 pad_maximum_fusion.2
  8.3 4.9 %collective-permute-start = (bf16[2,128,128]{2,1,0:T(8,128)(2,1)S(1)}, bf16[2,128,128]{2,1,0:T(8,128)(2,1)S(1)}, u32[]{:S(2)}, u32[]{:S(2)}) collective-permute-start(bf16[2,128,128]{2,1,0:T(8,128)(2,1)S(1)} %get-tuple-element.124), channel_id=1, source_target_pairs={{0,4},{4,8},{8,12},{12,16},{16,20},{20,24},{24,28},{1,5},{5,9},{9,... | collective-permute-start | bytes 196616 | tf_op jit(solution)/shard_map/ppermute | solution.py:20
  13.2 1.3 collective-permute-start.1
  14.5 0.6 collective-permute-done
  15.1 4.3 %collective-permute-done.1 = bf16[2,128,128]{2,1,0:T(8,128)(2,1)S(1)} collective-permute-done((bf16[2,128,128]{2,1,0:T(8,128)(2,1)S(1)}, bf16[2,128,128]{2,1,0:T(8,128)(2,1)S(1)}, u32[]{:S(2)}, u32[]{:S(2)}) %collective-permute-start.1) | collective-permute-done | bytes 65568 | tf_op jit(solution)/shard_map/ppermute | solution.py:22
  19.4 1.0 pad_maximum_fusion
  20.4 11.1 %while.12 = (s32[]{:T(128)}, bf16[2,256,512]{2,1,0:T(8,128)(2,1)}, bf16[2,768,128]{2,1,0:T(8,128)(2,1)S(1)}, s32[2]{0:T(128)S(1)}, s32[]{:T(128)}, /*index=5*/bf...) while((s32[]{:T(128)}, bf16[2,256,512]{2,1,0:T(8,128)(2,1)}, ...), condition=%wide.region_3.4_spmd, body=%wide.region_0.3_spmd.sunk | while | flops 273420544 | bytes 14467512 | solution.py:95
  20.4 0.6 dynamic_slice.42
  22.0 1.0 constant_dynamic-slice_fusion.2
  24.1 0.5 convolution_convert_fusion.4
  25.2 0.8 copy-done.3
  26.0 0.6 dynamic_slice.42
  27.6 1.0 constant_dynamic-slice_fusion.2
  30.7 0.8 copy-done.3
  31.5 3.6 convolution_convert_fusion.1
  37.0 50.9 %all-reduce.2.cloned.1.call-done = bf16[512,2048]{1,0:T(8,128)(2,1)} async-done(((bf16[512,2048]{1,0:T(8,128)(2,1)}), bf16[512,2048]{1,0:T(8,128)(2,1)}) %all-reduce.2.cloned.1.call-update) | async-done | bytes 2097168 | tf_op jit(solution)/shard_map/psum | solution.py:98
  87.9 4.9 %convert_add_fusion = (f32[512,2048]{1,0:T(8,128)}, f32[512]{0:T(512)S(1)}) fusion(bf16[512,2048]{1,0:T(8,128)(2,1)} %all-reduce.2.cloned.1.call-done, bf16[512,2048]{1,0:T(8,128)(2,1)} %param.16), kind=kLoop, calls=%fused_computation.25 | loop fusion | flops 5242368 | bytes 8390656 | tf_op jit(solution)/shard_map/add | solution.py:101
  92.8 38.4 %all-gather.4.cloned.1.call-done = bf16[2048,1408]{1,0:T(8,128)(2,1)} async-done(((bf16[256,1408]{1,0:T(8,128)(2,1)}), bf16[2048,1408]{1,0:T(8,128)(2,1)}) %all-gather.4.cloned.1.call-update) | async-done | bytes 5767184 | tf_op jit(solution)/shard_map/all_gather | solution.py:104
  131.2 9.0 %fusion.14 = f32[512,1408]{1,0:T(8,128)} fusion(bf16[2048,1408]{1,0:T(8,128)(2,1)} %all-gather.4.cloned.1.call-done, f32[2048]{0:T(1024)S(1)} %copy-done.4, f32[512]{0:T(512)S(1)} %add_rsqrt_fusion, bf16[512,2048]{1,0:T(8,128)(2,1)} %all-reduce.2.cloned.1.call-done, bf16[512,2048]{1,0:T(8,128)(2,1)} %param.16), kind=kOutput, calls=%fused_computation.36 | convolution fusion | flops 2959081472 | bytes 12855296 | tf_op jit(solution)/shard_map/dot_general | solution.py:106
  140.2 83.4 %all-gather.6.cloned.1.call-done = bf16[2048,1408]{1,0:T(8,128)(2,1)} async-done(((bf16[256,1408]{1,0:T(8,128)(2,1)}), bf16[2048,1408]{1,0:T(8,128)(2,1)}) %all-gather.6.cloned.1.call-update) | async-done | bytes 5767184 | tf_op jit(solution)/shard_map/all_gather | solution.py:105
  223.6 93.0 %all-gather.8.cloned.1.call-done = bf16[1408,2048]{1,0:T(8,128)(2,1)} async-done(((bf16[1408,256]{1,0:T(8,128)(2,1)}), bf16[1408,2048]{1,0:T(8,128)(2,1)}) %all-gather.8.cloned.1.call-update) | async-done | bytes 5767184 | tf_op jit(solution)/shard_map/all_gather | solution.py:61
  316.5 14.6 %convolution_convert_fusion.2 = bf16[512,2048]{1,0:T(8,128)(2,1)} fusion(bf16[1408,2048]{1,0:T(8,128)(2,1)} %all-gather.8.cloned.1.call-done, bf16[2048,1408]{1,0:T(8,128)(2,1)} %all-gather.6.cloned.1.call-done, f32[512,1408]{1,0:T(8,128)} %fusion.14, f32[2048]{0:T(1024)S(1)} %copy-done.4, f32[512]{0:T(512)S(1)} %add_rsqrt_fusion, ...), kind=kOutput, calls=%fused_computation.29 | convolution fusion | flops 5917245440 | bytes 20719616 | tf_op jit(solution)/shard_map/dot_general | solution.py:111
  331.2 29.5 %reduce-scatter.2.cloned.1.call-done = bf16[128,2048]{1,0:T(8,128)(2,1)} async-done(((bf16[512,2048]{1,0:T(8,128)(2,1)}), bf16[128,2048]{1,0:T(8,128)(2,1)}) %reduce-scatter.2.cloned.1.call-update) | async-done | bytes 524304 | tf_op jit(solution)/shard_map/reduce_scatter | solution.py:110
  360.7 2.3 add_convert_fusion
  (52 shorter events, 6.1 us)
Async XLA Ops:
  7.4 24.2 %copy-start = (bf16[512,2048]{1,0:T(8,128)(2,1)S(1)}, bf16[512,2048]{1,0:T(8,128)(2,1)}, u32[]{:S(2)}) copy-start(bf16[512,2048]{1,0:T(8,128)(2,1)} %param.18) | copy-start | bytes 6291460
  7.4 80.6 %all-reduce.2.cloned.1.call-start = ((), (), s32[]{:S(2)}) async-start(), calls=%async_computation.1 | async-start | bytes 4194304 | tf_op jit(solution)/shard_map/psum | solution.py:98
  8.3 6.8 %collective-permute-start = (bf16[2,128,128]{2,1,0:T(8,128)(2,1)S(1)}, bf16[2,128,128]{2,1,0:T(8,128)(2,1)S(1)}, u32[]{:S(2)}, u32[]{:S(2)}) collective-permute-start(bf16[2,128,128]{2,1,0:T(8,128)(2,1)S(1)} %get-tuple-element.124), channel_id=1, source_target_pairs={{0,4},{4,8},{8,12},{12,16},{16,20},{20,24},{24,28},{1,5},{5,9},{9,... | collective-permute-start | bytes 196616 | tf_op jit(solution)/shard_map/ppermute | solution.py:20
  13.2 6.2 %collective-permute-start.1 = (bf16[2,128,128]{2,1,0:T(8,128)(2,1)S(1)}, bf16[2,128,128]{2,1,0:T(8,128)(2,1)S(1)}, u32[]{:S(2)}, u32[]{:S(2)}) collective-permute-start(bf16[2,128,128]{2,1,0:T(8,128)(2,1)S(1)} %get-tuple-element.125), channel_id=1, source_target_pairs={{4,0},{8,4},{12,8},{16,12},{20,16},{24,20},{28,24},{5,1},{9,5},{13... | collective-permute-start | bytes 196616 | tf_op jit(solution)/shard_map/ppermute | solution.py:22
  20.4 3.2 copy-start.1
  24.1 1.0 copy-start.2
  25.2 0.8 copy-start.3
  26.0 3.2 copy-start.1
  29.7 1.0 copy-start.2
  30.7 0.8 copy-start.3
  35.2 96.0 %all-gather.4.cloned.1.call-start = ((), (), s32[]{:S(2)}) async-start(), calls=%async_computation.2 | async-start | bytes 6488064 | tf_op jit(solution)/shard_map/all_gather | solution.py:104
  35.8 187.8 %all-gather.6.cloned.1.call-start = ((), (), s32[]{:S(2)}) async-start(), calls=%async_computation.3 | async-start | bytes 6488064 | tf_op jit(solution)/shard_map/all_gather | solution.py:105
  36.4 280.2 %all-gather.8.cloned.1.call-start = ((), (), s32[]{:S(2)}) async-start(), calls=%async_computation.4 | async-start | bytes 6488064 | tf_op jit(solution)/shard_map/all_gather | solution.py:61
  37.0 94.3 %copy-start.4 = (f32[2048]{0:T(1024)S(1)}, f32[2048]{0:T(1024)}, u32[]{:S(2)}) copy-start(f32[2048]{0:T(1024)} %param.17) | copy-start | bytes 24580
  37.0 323.7 %reduce-scatter.2.cloned.1.call-start = ((), (), s32[]{:S(2)}) async-start(), calls=%async_computation.5 | async-start | bytes 2621440 | tf_op jit(solution)/shard_map/reduce_scatter | solution.py:110
Sparse Core Ops, SparseCore 0:
  35.3 52.5 all-reduce.1
  331.3 29.3 reduce-scatter.1
Sparse Core Ops, SparseCore 1:
  37.9 93.3 all-gather.3
  133.3 90.2 all-gather.5
  225.5 91.0 all-gather.7
where the time goes:
time: 371 us
  waiting for transfers between devices  302 us (81%)
  matrix products  29.2 us (8%)
  between operations  15.1 us (4%)
  other arithmetic  10.6 us (3%)
  starting transfers between devices  6.34 us (2%)
  local copies, waits for them, and re-layouts  6.13 us (2%)
    all_gather x1, waiting for transfers between devices, fetch_down(): return lax.all_gather(down_weight, 'sp', axis=1, tiled=True)  93 us
    all_gather x1, waiting for transfers between devices, shards(): up_sectioned = lax.all_gather(up_weight, 'sp', axis=0, tiled=True)  83.4 us
    psum x1, waiting for transfers between devices, shards(): lax.psum(jnp.dot(attended, out_weight, preferred_element_type=jnp.float32...  50.9 us
    all_gather x1, waiting for transfers between devices, shards(): gate_sectioned = lax.all_gather(gate_weight, 'sp', axis=0, tiled=True)  38.4 us
    reduce_scatter x1, waiting for transfers between devices, shards(): lax.psum_scatter(jnp.dot(hidden, down_whole, preferred_element_type=jnp.f...  29.5 us
    dot_general x1, matrix products, shards(): jnp.dot(hidden, down_whole, preferred_element_type=jnp.float32)  14.6 us
    dot_general x1, matrix products, shards(): jnp.dot(normed_all, gate_sectioned, preferred_element_type=jnp.float32)  8.96 us
  transfers between devices with their start and end apart: 7, of which 7 were waited for; matrix products, arithmetic and copies ran while one was open for 4% of the time, Pallas kernels for 0%

commit v1 on v0

--- a/solution.py
+++ b/solution.py
@@ -95,8 +95,9 @@
     blocks = lax.map(one_block, jnp.arange(tok_local // block_len, dtype=jnp.int32))
     attended = blocks.reshape(tok_local, queries.shape[1])
     own_first = lax.axis_index("tp") * share_rows
-    attn_full = lax.psum(
-        jnp.dot(attended, out_weight, preferred_element_type=jnp.float32).astype(jnp.bfloat16), "tp"
+    pack_the_ends = lambda u: jnp.sum(lax.all_gather(u, "tp"), 0)
+    attn_full = pack_the_ends(
+        jnp.dot(attended, out_weight, preferred_element_type=jnp.float32).astype(jnp.bfloat16)
     ).astype(jnp.float32)
     middle_all = residual.astype(jnp.float32) + attn_full
     normed_all = rms_scale(middle_all, norm_gain)

time: 371 us -> 428 us (1.15)
  waiting for transfers between devices: 302 us -> 353 us
  other arithmetic: 10.6 us -> 17.9 us
    all_gather x0 -> x1, waiting for transfers between devices: none -> 57.3 us  [shards(): pack_the_ends = lambda u: jnp.sum(lax.all_gather(u, 'tp'), 0)]
    psum x1 -> x0, waiting for transfers between devices: 50.9 us -> none  [shards(): lax.psum(jnp.dot(attended, out_weight, preferred_element_type=jnp.float32...]
    all_gather x1, waiting for transfers between devices: 38.4 us -> 82.4 us  [shards(): gate_sectioned = lax.all_gather(gate_weight, 'sp', axis=0, tiled=True)]
    all_gather x1, waiting for transfers between devices: 83.4 us -> 92.6 us  [shards(): up_sectioned = lax.all_gather(up_weight, 'sp', axis=0, tiled=True)]
    all_gather x1, waiting for transfers between devices: 93 us -> 84.5 us  [fetch_down(): return lax.all_gather(down_weight, 'sp', axis=1, tiled=True)]
    reduce_sum x0 -> x1, other arithmetic: none -> 7.22 us  [shards(): pack_the_ends = lambda u: jnp.sum(lax.all_gather(u, 'tp'), 0)]
  transfers between devices with their start and end apart: 7 -> 7, of which waited for: 7 -> 7; matrix products, arithmetic and copies ran while one was open for 4% -> 5% of each run, Pallas kernels for 0% -> 0%
where the time goes in v1:
time: 428 us; the launch traced here: 427 us
  waiting for transfers between devices  353 us (82%)
  matrix products  29.1 us (7%)
  other arithmetic  17.9 us (4%)
  between operations  13.2 us (3%)
  starting transfers between devices  6.5 us (2%)
  local copies, waits for them, and re-layouts  6.13 us (1%)
    all_gather x1, waiting for transfers between devices, shards(): up_sectioned = lax.all_gather(up_weight, 'sp', axis=0, tiled=True)  92.6 us
    all_gather x1, waiting for transfers between devices, fetch_down(): return lax.all_gather(down_weight, 'sp', axis=1, tiled=True)  84.5 us
    all_gather x1, waiting for transfers between devices, shards(): gate_sectioned = lax.all_gather(gate_weight, 'sp', axis=0, tiled=True)  82.4 us
    all_gather x1, waiting for transfers between devices, shards(): pack_the_ends = lambda u: jnp.sum(lax.all_gather(u, 'tp'), 0)  57.3 us
    reduce_scatter x1, waiting for transfers between devices, shards(): lax.psum_scatter(jnp.dot(hidden, down_whole, preferred_element_type=jnp.f...  29.5 us
    dot_general x1, matrix products, shards(): jnp.dot(hidden, down_whole, preferred_element_type=jnp.float32)  14.5 us
    dot_general x1, matrix products, shards(): jnp.dot(normed_all, gate_sectioned, preferred_element_type=jnp.float32)  8.96 us
  transfers between devices with their start and end apart: 7, of which 7 were waited for; matrix products, arithmetic and copies ran while one was open for 5% of the time, Pallas kernels for 0%

profile of v1, /device:TPU:0, one launch (start us, length us, event | category | flops | bytes accessed | tf_op | source)
XLA Modules:
  0.0 427.3 jit_solution(3487236097310128484)
XLA Ops:
  6.5 1.0 pad_maximum_fusion.2
  7.5 4.9 %collective-permute-start = (bf16[2,128,128]{2,1,0:T(8,128)(2,1)S(1)}, bf16[2,128,128]{2,1,0:T(8,128)(2,1)S(1)}, u32[]{:S(2)}, u32[]{:S(2)}) collective-permute-start(bf16[2,128,128]{2,1,0:T(8,128)(2,1)S(1)} %get-tuple-element.124), channel_id=1, source_target_pairs={{0,4},{4,8},{8,12},{12,16},{16,20},{20,24},{24,28},{1,5},{5,9},{9,... | collective-permute-start | bytes 196616 | tf_op jit(solution)/shard_map/ppermute | solution.py:20
  12.4 1.3 collective-permute-start.1
  14.3 4.3 %collective-permute-done.1 = bf16[2,128,128]{2,1,0:T(8,128)(2,1)S(1)} collective-permute-done((bf16[2,128,128]{2,1,0:T(8,128)(2,1)S(1)}, bf16[2,128,128]{2,1,0:T(8,128)(2,1)S(1)}, u32[]{:S(2)}, u32[]{:S(2)}) %collective-permute-start.1) | collective-permute-done | bytes 65568 | tf_op jit(solution)/shard_map/ppermute | solution.py:22
  18.6 1.0 pad_maximum_fusion
  19.6 11.1 %while.12 = (s32[]{:T(128)}, bf16[2,256,512]{2,1,0:T(8,128)(2,1)}, bf16[2,768,128]{2,1,0:T(8,128)(2,1)S(1)}, s32[2]{0:T(128)S(1)}, s32[]{:T(128)}, /*index=5*/bf...) while((s32[]{:T(128)}, bf16[2,256,512]{2,1,0:T(8,128)(2,1)}, ...), condition=%wide.region_3.4_spmd, body=%wide.region_0.3_spmd.sunk | while | flops 273420544 | bytes 14467512 | solution.py:95
  19.6 0.6 dynamic_slice.42
  21.2 1.0 constant_dynamic-slice_fusion.2
  24.4 0.8 copy-done.3
  26.7 1.0 constant_dynamic-slice_fusion.2
  29.9 0.8 copy-done.3
  30.7 3.6 convolution_convert_fusion.1
  34.4 0.7 all-gather.6.cloned.1.call-update
  35.2 0.7 all-gather.10.cloned.1.call-update
  36.6 57.3 %all-gather.12.cloned.1.call-done = bf16[2048,2048]{1,0:T(8,128)(2,1)} async-done(((bf16[512,2048]{1,0:T(8,128)(2,1)}), bf16[2048,2048]{1,0:T(8,128)(2,1)}) %all-gather.12.cloned.1.call-update) | async-done | bytes 8388624 | tf_op jit(solution)/shard_map/all_gather | solution.py:98
  94.0 7.2 %reduce_sum.30 = bf16[512,2048]{1,0:T(8,128)(2,1)} reduce(bf16[4,512,2048]{2,1,0:T(8,128)(2,1)} %bitcast.50, bf16[]{:T(256)} %constant.90.clone.1), dimensions={0}, to_apply=%region_4.5 | reduce | flops 3145728 | bytes 10485762 | tf_op jit(solution)/shard_map/reduce_sum | solution.py:98
  101.2 4.9 %convert_add_fusion = (f32[512,2048]{1,0:T(8,128)}, f32[512]{0:T(512)S(1)}) fusion(bf16[512,2048]{1,0:T(8,128)(2,1)} %reduce_sum.30, bf16[512,2048]{1,0:T(8,128)(2,1)} %param.16), kind=kLoop, calls=%fused_computation.25 | loop fusion | flops 5242368 | bytes 8390656 | tf_op jit(solution)/shard_map/add | solution.py:102
  106.1 82.4 %all-gather.6.cloned.1.call-done = bf16[2048,1408]{1,0:T(8,128)(2,1)} async-done(((bf16[256,1408]{1,0:T(8,128)(2,1)}), bf16[2048,1408]{1,0:T(8,128)(2,1)}) %all-gather.6.cloned.1.call-update) | async-done | bytes 5767184 | tf_op jit(solution)/shard_map/all_gather | solution.py:105
  188.5 9.0 %fusion.14 = f32[512,1408]{1,0:T(8,128)} fusion(bf16[2048,1408]{1,0:T(8,128)(2,1)} %all-gather.6.cloned.1.call-done, f32[2048]{0:T(1024)S(1)} %copy-done.4, f32[512]{0:T(512)S(1)} %add_rsqrt_fusion, bf16[512,2048]{1,0:T(8,128)(2,1)} %reduce_sum.30, bf16[512,2048]{1,0:T(8,128)(2,1)} %param.16), kind=kOutput, calls=%fused_computation.36 | convolution fusion | flops 2959081472 | bytes 12855296 | tf_op jit(solution)/shard_map/dot_general | solution.py:107
  197.5 84.5 %all-gather.10.cloned.1.call-done = bf16[1408,2048]{1,0:T(8,128)(2,1)} async-done(((bf16[1408,256]{1,0:T(8,128)(2,1)}), bf16[1408,2048]{1,0:T(8,128)(2,1)}) %all-gather.10.cloned.1.call-update) | async-done | bytes 5767184 | tf_op jit(solution)/shard_map/all_gather | solution.py:61
  281.9 92.6 %all-gather.8.cloned.1.call-done = bf16[2048,1408]{1,0:T(8,128)(2,1)} async-done(((bf16[256,1408]{1,0:T(8,128)(2,1)}), bf16[2048,1408]{1,0:T(8,128)(2,1)}) %all-gather.8.cloned.1.call-update) | async-done | bytes 5767184 | tf_op jit(solution)/shard_map/all_gather | solution.py:106
  374.5 14.5 %convolution_convert_fusion.2 = bf16[512,2048]{1,0:T(8,128)(2,1)} fusion(bf16[1408,2048]{1,0:T(8,128)(2,1)} %all-gather.10.cloned.1.call-done, bf16[2048,1408]{1,0:T(8,128)(2,1)} %all-gather.8.cloned.1.call-done, f32[512,1408]{1,0:T(8,128)} %fusion.14, f32[2048]{0:T(1024)S(1)} %copy-done.4, f32[512]{0:T(512)S(1)} %add_rsqrt_fusion, ...), kind=kOutput, calls=%fused_computation.29 | convolution fusion | flops 5917245440 | bytes 20719616 | tf_op jit(solution)/shard_map/dot_general | solution.py:112
  389.0 29.5 %reduce-scatter.2.cloned.1.call-done = bf16[128,2048]{1,0:T(8,128)(2,1)} async-done(((bf16[512,2048]{1,0:T(8,128)(2,1)}), bf16[128,2048]{1,0:T(8,128)(2,1)}) %reduce-scatter.2.cloned.1.call-update) | async-done | bytes 524304 | tf_op jit(solution)/shard_map/reduce_scatter | solution.py:111
  418.5 2.3 add_convert_fusion
  (53 shorter events, 7.0 us)
Async XLA Ops:
  6.5 24.2 %copy-start = (bf16[512,2048]{1,0:T(8,128)(2,1)S(1)}, bf16[512,2048]{1,0:T(8,128)(2,1)}, u32[]{:S(2)}) copy-start(bf16[512,2048]{1,0:T(8,128)(2,1)} %param.18) | copy-start | bytes 6291460
  6.5 87.4 %all-gather.12.cloned.1.call-start = ((), (), s32[]{:S(2)}) async-start(), calls=%async_computation.5 | async-start | bytes 10485760 | tf_op jit(solution)/shard_map/all_gather | solution.py:98
  7.5 6.8 %collective-permute-start = (bf16[2,128,128]{2,1,0:T(8,128)(2,1)S(1)}, bf16[2,128,128]{2,1,0:T(8,128)(2,1)S(1)}, u32[]{:S(2)}, u32[]{:S(2)}) collective-permute-start(bf16[2,128,128]{2,1,0:T(8,128)(2,1)S(1)} %get-tuple-element.124), channel_id=1, source_target_pairs={{0,4},{4,8},{8,12},{12,16},{16,20},{20,24},{24,28},{1,5},{5,9},{9,... | collective-permute-start | bytes 196616 | tf_op jit(solution)/shard_map/ppermute | solution.py:20
  12.4 6.2 %collective-permute-start.1 = (bf16[2,128,128]{2,1,0:T(8,128)(2,1)S(1)}, bf16[2,128,128]{2,1,0:T(8,128)(2,1)S(1)}, u32[]{:S(2)}, u32[]{:S(2)}) collective-permute-start(bf16[2,128,128]{2,1,0:T(8,128)(2,1)S(1)} %get-tuple-element.125), channel_id=1, source_target_pairs={{4,0},{8,4},{12,8},{16,12},{20,16},{24,20},{28,24},{5,1},{9,5},{13... | collective-permute-start | bytes 196616 | tf_op jit(solution)/shard_map/ppermute | solution.py:22
  19.6 3.2 copy-start.1
  23.3 1.0 copy-start.2
  24.3 0.8 copy-start.3
  25.1 3.2 copy-start.1
  28.8 1.0 copy-start.2
  29.9 0.8 copy-start.3
  34.4 154.1 %all-gather.6.cloned.1.call-start = ((), (), s32[]{:S(2)}) async-start(), calls=%async_computation.1 | async-start | bytes 6488064 | tf_op jit(solution)/shard_map/all_gather | solution.py:105
  35.1 246.8 %all-gather.10.cloned.1.call-start = ((), (), s32[]{:S(2)}) async-start(), calls=%async_computation.3 | async-start | bytes 6488064 | tf_op jit(solution)/shard_map/all_gather | solution.py:61
  35.8 338.6 %all-gather.8.cloned.1.call-start = ((), (), s32[]{:S(2)}) async-start(), calls=%async_computation.2 | async-start | bytes 6488064 | tf_op jit(solution)/shard_map/all_gather | solution.py:106
  36.4 382.1 %reduce-scatter.2.cloned.1.call-start = ((), (), s32[]{:S(2)}) async-start(), calls=%async_computation.4 | async-start | bytes 2621440 | tf_op jit(solution)/shard_map/reduce_scatter | solution.py:111
  101.2 87.3 %copy-start.4 = (f32[2048]{0:T(1024)S(1)}, f32[2048]{0:T(1024)}, u32[]{:S(2)}) copy-start(f32[2048]{0:T(1024)} %param.17) | copy-start | bytes 24580
Sparse Core Ops, SparseCore 0:
  34.5 59.4 all-gather.11
  96.2 92.2 all-gather.5
  190.5 91.3 all-gather.9
  283.9 90.4 all-gather.7
  389.1 29.3 reduce-scatter.1
